TPU v7x, 32 devices: a whole 2x2x4 slice. The times are simulated.
32 devices in a mesh: fs: 8 (over z, y), tp: 4 (over x, core).
Axes of the slice: x: 2, y: 2, z: 4, core: 2. Of those that a mesh axis runs over, the one named last changes fastest.
Arguments:
- tokens: bfloat16 [3072, 2048], P('tp'), may hold values from -6 to 6
- norm_gain: float32 [2048], P('fs'), may hold values from 0.1 to 1.9
- gate_weight: float32 [4, 2048, 8192], P(None, 'fs', 'tp'), may hold values from -0.125 to 0.125
- up_weight: float32 [4, 2048, 8192], P(None, 'fs', 'tp'), may hold values from -0.125 to 0.125
- down_weight: float32 [4, 8192, 2048], P(None, 'fs', 'tp'), may hold values from -0.0625 to 0.0625
- routes: int32 [3072, 2], P('tp'), may hold values from 0 to 3, all different within a row; in each aligned block of 768 rows (0 to 767, 768 to 1535, ...) at most 480 rows name the same one
- route_logit: float32 [3072, 2], P('tp'), may hold values from -6 to 6
Outputs:
- gate_out: bfloat16 [4, 2048, 8192], P(None, None, 'fs')
- up_out: bfloat16 [4, 2048, 8192], P(None, None, 'fs')
- down_out: bfloat16 [4, 8192, 2048], P(None, 'fs')
- mixed: bfloat16 [3072, 2048], P(('tp', 'fs'))
Inputs may be any that keep to these rules, and one draw needn't show every extreme that they name: `routes`: the two experts of a token differ. In each aligned block of 768 tokens (the tokens of one request group) every expert is named by at most 480 tokens, a bound that some block reaches.
All inputs are finite; a program needn't handle non-finite values.
Results may differ from a plain program's by a relative error of at most 0.0082.
Values may be sent and summed in bfloat16 or wider, within the bound.
No kernel may reach another device: no remote copies, remote signals or barrier semaphores. Data moves between devices by JAX's collectives and lax.ppermute only.
A program may use at most 192 MiB of HBM per device.

v0:
```python
import jax
import jax.numpy as jnp
from jax import lax
from jax.sharding import PartitionSpec as P

EPS = 0.5


def shards(tokens, norm_gain, gate_weight, up_weight, down_weight, routes, route_logit):
    gain_col = norm_gain[None, :, None]
    gate_part = (gate_weight * gain_col).astype(jnp.bfloat16)
    up_part = (up_weight * gain_col).astype(jnp.bfloat16)
    down_part = down_weight.astype(jnp.bfloat16)
    gate_one, up_one = (
        lax.all_to_all(gate_part, "tp", split_axis=0, concat_axis=2, tiled=True),
        lax.all_to_all(up_part, "tp", split_axis=0, concat_axis=2, tiled=True),
    )
    gate_mine, up_mine = (
        lax.all_to_all(gate_one, "fs", split_axis=2, concat_axis=1, tiled=True),
        lax.all_to_all(up_one, "fs", split_axis=2, concat_axis=1, tiled=True),
    )
    gate_out, up_out = (
        lax.all_gather(gate_mine, "tp", axis=0, tiled=True),
        lax.all_gather(up_mine, "tp", axis=0, tiled=True),
    )
    down_out = lax.all_gather(down_part, "tp", axis=2, tiled=True)
    total_rows = tokens.shape[0]
    width = tokens.shape[1]
    experts = gate_out.shape[0]
    capacity = total_rows * 5 // 8
    floats = tokens.astype(jnp.float32)
    normed = (floats * lax.rsqrt(jnp.mean(floats * floats, axis=1, keepdims=True) + EPS)).astype(
        jnp.bfloat16
    )
    first_share = jax.nn.sigmoid(route_logit[:, 0] - route_logit[:, 1])
    shares = jnp.stack([first_share, 1.0 - first_share], axis=1)
    chosen = (routes[:, :, None] == jnp.arange(experts, dtype=jnp.int32)[None, None, :]).astype(
        jnp.int32
    )
    counts = jnp.sum(chosen, axis=1)
    before = jnp.cumsum(counts, axis=0) - counts
    slot_index = jnp.sum(chosen * before[:, None, :], axis=2)
    flat_slot = routes * capacity + slot_index
    row_ids = jnp.repeat(jnp.arange(total_rows, dtype=jnp.int32), 2)
    table = (
        jnp.full((experts * capacity,), total_rows, jnp.int32)
        .at[flat_slot.reshape(-1)]
        .set(row_ids)
    )
    gathered = jnp.take(normed, table, axis=0, mode="fill", fill_value=0).reshape(
        experts, capacity, width
    )
    gate_val = jnp.einsum("ecd,edf->ecf", gathered, gate_out, preferred_element_type=jnp.float32)
    up_val = jnp.einsum("ecd,edf->ecf", gathered, up_out, preferred_element_type=jnp.float32)
    hidden = (jax.nn.silu(gate_val) * up_val).astype(jnp.bfloat16)
    results = jnp.einsum("ecf,efd->ecd", hidden, down_out, preferred_element_type=jnp.float32)
    flat_rows = results.reshape(experts * capacity, width)
    first_rows = jnp.take(flat_rows, flat_slot[:, 0], axis=0)
    second_rows = jnp.take(flat_rows, flat_slot[:, 1], axis=0)
    mixed = lax.psum_scatter(
        shares[:, 0:1] * first_rows + shares[:, 1:2] * second_rows,
        "fs",
        scatter_dimension=0,
        tiled=True,
    )
    return (gate_out, up_out, down_out, mixed.astype(jnp.bfloat16))


def solution(mesh):
    return jax.shard_map(
        shards,
        mesh=mesh,
        in_specs=(
            P("tp", None),
            P("fs"),
            P(None, "fs", "tp"),
            P(None, "fs", "tp"),
            P(None, "fs", "tp"),
            P("tp", None),
            P("tp", None),
        ),
        out_specs=(
            P(None, None, "fs"),
            P(None, None, "fs"),
            P(None, "fs", None),
            P(("tp", "fs"), None),
        ),
        check_vma=False,
    )
```

profile of v0, /device:TPU:0, one launch (start us, length us, event | category | flops | bytes accessed | tf_op | source)
XLA Modules:
  0.0 959.0 jit_solution(9687158230475078291)
XLA Ops:
  7.2 8.7 copy.43
  15.9 8.7 copy.46
  24.6 10.7 %multiply_convert_fusion = (bf16[4,256,2048]{1,2,0:T(8,128)(2,1)}, bf16[4,256,2048]{1,2,0:T(8,128)(2,1)}) fusion(f32[4,256,2048]{1,2,0:T(8,128)} %copy.46, f32[256]{0:T(256)S(1)} %copy-done.3, f32[4,256,2048]{1,2,0:T(8,128)} %copy.43), kind=kLoop, calls=%fused_computation.4 | loop fusion | flops 8388608 | bytes 25166848 | tf_op jit(solution)/shard_map/convert_element_type | solution.py:12
  35.3 52.6 %all_to_all.72 = bf16[4,256,2048]{1,2,0:T(8,128)(2,1)S(1)} all-to-all(bf16[4,256,2048]{1,2,0:T(8,128)(2,1)} %get-tuple-element.9), channel_id=1, replica_groups=mesh['fs'=8,'tp'=4] {'tp'}, dimensions={0} | all-to-all | bytes 8388608 | tf_op jit(solution)/shard_map/all_to_all | solution.py:16
  87.9 49.3 %copy.56 = bf16[1,256,8192]{1,0,2:T(2,128)(2,1)} copy(bf16[1,256,8192]{1,2,0:T(8,128)(2,1)S(1)} %bitcast.49) | data formatting | bytes 8388608 | tf_op jit(solution)/shard_map/all_to_all | solution.py:16
  137.7 43.5 %reduce.13 = bf16[8192,256]{1,0:T(8,128)(2,1)} reduce(bf16[8192,1,256]{2,1,0:T(2,128)(2,1)} %bitcast.45, bf16[]{:T(256)} %broadcast.78), dimensions={1}, to_apply=%bitcast.40.reduce_sub_computation | reduce | bytes 8388610
  181.2 6.9 reshape.137
  188.2 99.8 %all_to_all.73 = bf16[8,2,131072]{2,1,0:T(2,128)(2,1)} all-to-all(bf16[8,2,131072]{2,1,0:T(2,128)(2,1)} %reshape.137), channel_id=1, replica_groups=mesh['fs'=8,'tp'=4] {'fs'}, dimensions={0} | all-to-all | bytes 8388608 | tf_op jit(solution)/shard_map/all_to_all | solution.py:20
  288.0 8.7 reshape.138
  296.7 6.1 copy.51
  302.8 6.4 copy.48
  309.3 6.0 convert_element_type.26
  315.4 97.4 %all_to_all.74 = bf16[4,256,2048]{1,2,0:T(8,128)(2,1)S(1)} all-to-all(bf16[4,256,2048]{1,2,0:T(8,128)(2,1)} %get-tuple-element.10), channel_id=1, replica_groups=mesh['fs'=8,'tp'=4] {'tp'}, dimensions={0} | all-to-all | bytes 8388608 | tf_op jit(solution)/shard_map/all_to_all | solution.py:15
  412.8 49.3 %copy.57 = bf16[1,256,8192]{1,0,2:T(2,128)(2,1)} copy(bf16[1,256,8192]{1,2,0:T(8,128)(2,1)S(1)} %bitcast.51) | data formatting | bytes 8388608 | tf_op jit(solution)/shard_map/all_to_all | solution.py:15
  462.2 43.5 %reduce.12 = bf16[8192,256]{1,0:T(8,128)(2,1)} reduce(bf16[8192,1,256]{2,1,0:T(2,128)(2,1)} %bitcast.46, bf16[]{:T(256)} %broadcast.78), dimensions={1}, to_apply=%bitcast.41.reduce_sub_computation | reduce | bytes 8388610
  505.7 7.0 reshape.135
  512.7 97.7 %all_to_all.75 = bf16[8,2,131072]{2,1,0:T(2,128)(2,1)} all-to-all(bf16[8,2,131072]{2,1,0:T(2,128)(2,1)} %reshape.135), channel_id=1, replica_groups=mesh['fs'=8,'tp'=4] {'fs'}, dimensions={0} | all-to-all | bytes 8388608 | tf_op jit(solution)/shard_map/all_to_all | solution.py:19
  610.4 8.7 reshape.136
  619.1 6.1 copy.50
  625.2 6.6 copy.45
  634.9 6.3 scatter_custom_fusion
  644.9 8.9 gather_fusion
  654.0 16.3 %fusion = f32[4,480,1024]{2,1,0:T(8,128)} fusion(bf16[4,2048,1024]{2,1,0:T(8,128)(2,1)} %all-gather.6.cloned.1.call-done, bf16[4,480,2048]{2,1,0:T(8,128)(2,1)} %bitcast.57, pred[4,480]{1,0:T(4,128)(4,1)S(1)} %broadcast_in_dim.37), kind=kOutput, calls=%fused_computation.10 | convolution fusion | flops 8056995840 | bytes 32507776 | tf_op jit(solution)/shard_map/ecd,edf->ecf/dot_general | solution.py:54
  670.2 65.7 %all-gather.4.cloned.1.call-done = bf16[4,2048,1024]{2,1,0:T(8,128)(2,1)} async-done(((bf16[1,2048,1024]{2,1,0:T(8,128)(2,1)}), bf16[4,2048,1024]{2,1,0:T(8,128)(2,1)}) %all-gather.4.cloned.1.call-update) | async-done | bytes 16777232 | tf_op jit(solution)/shard_map/all_gather | solution.py:23
  735.9 27.2 %fusion.7 = f32[4,480,2048]{2,1,0:T(8,128)} fusion(bf16[4,1024,2048]{2,1,0:T(8,128)(2,1)} %all-gather.8.cloned.1.call-done, f32[4,480,1024]{2,1,0:T(8,128)} %fusion, bf16[4,2048,1024]{2,1,0:T(8,128)(2,1)} %all-gather.4.cloned.1.call-done, bf16[4,480,2048]{2,1,0:T(8,128)(2,1)} %bitcast.58, pred[4,480]{1,0:T(4,128)(4,1)S(1)} %broadcast_in_dim.37), kind=kOutput, calls=%fused_computation.19 | convolution fusion | flops 16121856000 | bytes 65013632 | tf_op jit(solution)/shard_map/ecf,efd->ecd/dot_general | solution.py:56
  763.1 12.7 %gather_fusion.1 = f32[768,2048]{1,0:T(8,128)} fusion(f32[1920,2048]{1,0:T(8,128)} %bitcast.43, s32[1024]{0:T(1024)S(1)} %pad_clamp_fusion.2), kind=kCustom, calls=%fused_computation.clone | custom fusion | bytes 12585984 | tf_op jit(solution)/shard_map/jit(_take)/gather | solution.py:58
  775.8 12.7 %gather_fusion.2 = f32[768,2048]{1,0:T(8,128)} fusion(f32[1920,2048]{1,0:T(8,128)} %bitcast.44, s32[1024]{0:T(1024)S(1)} %pad_clamp_fusion.1), kind=kCustom, calls=%fused_computation.1.clone | custom fusion | bytes 12585984 | tf_op jit(solution)/shard_map/jit(_take)/gather | solution.py:59
  788.5 7.2 fusion.4
  795.7 118.2 %reduce-scatter.2.cloned.1.call-done = f32[96,2048]{1,0:T(8,128)} async-done(((f32[768,2048]{1,0:T(8,128)}), f32[96,2048]{1,0:T(8,128)}) %reduce-scatter.2.cloned.1.call-update) | async-done | bytes 786448 | tf_op jit(solution)/shard_map/reduce_scatter | solution.py:60
  915.8 15.2 %copy.61 = bf16[4,2048,1024]{2,1,0:T(8,128)(2,1)} copy(bf16[4,2048,1024]{2,1,0:T(8,128)(2,1)} %all-gather.4.cloned.1.call-done) | data formatting | bytes 33554432
  931.1 15.2 %copy.62 = bf16[4,2048,1024]{2,1,0:T(8,128)(2,1)} copy(bf16[4,2048,1024]{2,1,0:T(8,128)(2,1)} %all-gather.6.cloned.1.call-done) | data formatting | bytes 33554432
  946.3 6.2 copy.63
  (56 shorter events, 9.4 us)
Async XLA Ops:
  7.2 646.8 %all-gather.6.cloned.1.call-start = ((), (), s32[]{:S(2)}) async-start(), calls=%async_computation.6 | async-start | bytes 20971520 | tf_op jit(solution)/shard_map/all_gather | solution.py:24
  15.9 8.7 copy-start.3
  309.3 360.9 %all-gather.8.cloned.1.call-start = ((), (), s32[]{:S(2)}) async-start(), calls=%async_computation.7 | async-start | bytes 20971520 | tf_op jit(solution)/shard_map/all_gather | solution.py:26
  315.4 420.5 %all-gather.4.cloned.1.call-start = ((), (), s32[]{:S(2)}) async-start(), calls=%async_computation.5 | async-start | bytes 20971520 | tf_op jit(solution)/shard_map/all_gather | solution.py:23
  625.2 6.7 copy-start.1
  625.2 16.2 %copy-start = (bf16[768,2048]{1,0:T(8,128)(2,1)S(1)}, bf16[768,2048]{1,0:T(8,128)(2,1)}, u32[]{:S(2)}) copy-start(bf16[768,2048]{1,0:T(8,128)(2,1)} %param.9) | copy-start | bytes 9437188
  631.8 282.1 %reduce-scatter.2.cloned.1.call-start = ((), (), s32[]{:S(2)}) async-start(), calls=%async_computation.8 | async-start | bytes 7077888 | tf_op jit(solution)/shard_map/reduce_scatter | solution.py:60
  644.9 8.9 copy-start.2
  915.8 30.5 %slice-start = ((s8[16777216]{0:T(1024)(128)(4,1)}), s8[4194304]{0:T(1024)(128)(4,1)S(1)}, s32[]{:S(2)}) async-start(s8[16777216]{0:T(1024)(128)(4,1)} %bitcast.53), calls=%async_computation.9 | async-start | bytes 8388608
  915.8 30.5 %slice-start.1 = ((s8[16777216]{0:T(1024)(128)(4,1)}), s8[4194304]{0:T(1024)(128)(4,1)S(1)}, s32[]{:S(2)}) async-start(s8[16777216]{0:T(1024)(128)(4,1)} %bitcast.53), calls=%async_computation.10 | async-start | bytes 8388608
  931.1 15.2 %slice-start.2 = ((s8[16777216]{0:T(1024)(128)(4,1)}), s8[4194304]{0:T(1024)(128)(4,1)S(1)}, s32[]{:S(2)}) async-start(s8[16777216]{0:T(1024)(128)(4,1)} %bitcast.53), calls=%async_computation.11 | async-start | bytes 8388608
  931.1 15.2 %slice-start.3 = ((s8[16777216]{0:T(1024)(128)(4,1)}), s8[4194304]{0:T(1024)(128)(4,1)S(1)}, s32[]{:S(2)}) async-start(s8[16777216]{0:T(1024)(128)(4,1)} %bitcast.53), calls=%async_computation.12 | async-start | bytes 8388608
Sparse Core Ops, SparseCore 0:
  309.4 148.9 all-gather.5
  460.0 104.8 all-gather.7
  631.9 103.9 all-gather.3
  795.8 118.0 reduce-scatter.1
where the time goes:
time: 961 us; the launch traced here: 959 us
  blocking collectives  347 us (36%)
  local copies, waits for them, and re-layouts  252 us (26%)
  waiting for transfers between devices  184 us (19%)
  other arithmetic  118 us (12%)
  matrix products  43.5 us (5%)
  between operations  14 us (1%)
    reduce_scatter x1, waiting for transfers between devices, shards(): lax.psum_scatter(shares[:, 0:1] * first_rows + shares[:, 1:2] * second_ro...  118 us
    all_to_all x1, blocking collectives, shards(): lax.all_to_all(up_one, 'fs', split_axis=2, concat_axis=1, tiled=True)  99.8 us
    unnamed x28, local copies, waits for them, and re-layouts  98.2 us
    all_to_all x1, blocking collectives, shards(): lax.all_to_all(gate_one, 'fs', split_axis=2, concat_axis=1, tiled=True)  97.7 us
    all_to_all x1, blocking collectives, shards(): lax.all_to_all(gate_part, 'tp', split_axis=0, concat_axis=2, tiled=True)  97.4 us
    unnamed x4, other arithmetic  87.2 us
    all_gather x1, waiting for transfers between devices, shards(): lax.all_gather(gate_mine, 'tp', axis=0, tiled=True)  65.7 us
    all_to_all x1, blocking collectives, shards(): lax.all_to_all(up_part, 'tp', split_axis=0, concat_axis=2, tiled=True)  52.6 us
  transfers between devices with their start and end apart: 4, of which 2 were waited for; matrix products, arithmetic and copies ran while one was open for 17% of the time, Pallas kernels for 0%

commit v1 on v0

--- a/solution.py
+++ b/solution.py
@@ -4,6 +4,18 @@
 from jax.sharding import PartitionSpec as P
 
 EPS = 0.5
+
+
+def sent_to_each(x, axis, split, join):
+    ways, here = (lax.axis_size(axis), lax.axis_index(axis))
+    width = x.shape[split] // ways
+    turned = jnp.roll(x, -here * width, axis=split)
+    got = [lax.slice_in_dim(turned, 0, width, axis=split)]
+    for far in range(1, ways):
+        sent = lax.slice_in_dim(turned, far * width, (far + 1) * width, axis=split)
+        got.append(lax.ppermute(sent, axis, [(d, (d + far) % ways) for d in range(ways)]))
+    line = jnp.concatenate(got[::-1], axis=join)
+    return jnp.roll(line, (here + 1) * got[0].shape[join], axis=join)
 
 
 def shards(tokens, norm_gain, gate_weight, up_weight, down_weight, routes, route_logit):
@@ -16,7 +28,7 @@
         lax.all_to_all(up_part, "tp", split_axis=0, concat_axis=2, tiled=True),
     )
     gate_mine, up_mine = (
-        lax.all_to_all(gate_one, "fs", split_axis=2, concat_axis=1, tiled=True),
+        sent_to_each(gate_one, "fs", 2, 1),
         lax.all_to_all(up_one, "fs", split_axis=2, concat_axis=1, tiled=True),
     )
     gate_out, up_out = (

time: 961 us -> 898 us (0.934)
  waiting for transfers between devices: 184 us -> 407 us
  blocking collectives: 347 us -> 152 us
  local copies, waits for them, and re-layouts: 252 us -> 189 us
  other arithmetic: 118 us -> 77.4 us
  starting transfers between devices: 0.16 us -> 13.2 us
    all_to_all x2 -> x0, blocking collectives: 195 us -> none  [the longest x1 97.7 us: shards(): lax.all_to_all(gate_one, 'fs', split_axis=2, concat_axis=1, tiled=True)]
    all_to_all x0 -> x1, waiting for transfers between devices: none -> 93.3 us  [shards(): lax.all_to_all(gate_part, 'tp', split_axis=0, concat_axis=2, tiled=True)]
    ppermute x0 -> x7, waiting for transfers between devices: none -> 85.6 us  [sent_to_each(): lax.ppermute(sent, axis, [(d, (d + far) % ways) for d in range(ways)])]
    unnamed x4 -> x3, other arithmetic: 87.2 us -> 43.6 us
    all_to_all x1, local copies, waits for them, and re-layouts: 49.3 us -> 6.32 us  [shards(): lax.all_to_all(gate_part, 'tp', split_axis=0, concat_axis=2, tiled=True)]
    all_gather x1, waiting for transfers between devices: 65.7 us -> 108 us  [shards(): lax.all_gather(gate_mine, 'tp', axis=0, tiled=True)]
    unnamed x28 -> x42, local copies, waits for them, and re-layouts: 98.2 us -> 79.9 us
  transfers between devices with their start and end apart: 4 -> 12, of which waited for: 2 -> 9; matrix products, arithmetic and copies ran while one was open for 17% -> 7% of each run, Pallas kernels for 0% -> 0%
where the time goes in v1:
time: 898 us; the launch traced here: 897 us
  waiting for transfers between devices  407 us (45%)
  local copies, waits for them, and re-layouts  189 us (21%)
  blocking collectives  152 us (17%)
  other arithmetic  77.4 us (9%)
  matrix products  43.4 us (5%)
  between operations  14.1 us (2%)
  starting transfers between devices  13.2 us (1%)
    reduce_scatter x1, waiting for transfers between devices, shards(): lax.psum_scatter(shares[:, 0:1] * first_rows + shares[:, 1:2] * second_ro...  118 us
    all_gather x1, waiting for transfers between devices, shards(): lax.all_gather(gate_mine, 'tp', axis=0, tiled=True)  108 us
    all_to_all x1, blocking collectives, shards(): lax.all_to_all(up_one, 'fs', split_axis=2, concat_axis=1, tiled=True)  99.8 us
    all_to_all x1, waiting for transfers between devices, shards(): lax.all_to_all(gate_part, 'tp', split_axis=0, concat_axis=2, tiled=True)  93.3 us
    ppermute x7, waiting for transfers between devices, sent_to_each(): lax.ppermute(sent, axis, [(d, (d + far) % ways) for d in range(ways)])  85.6 us
    unnamed x42, local copies, waits for them, and re-layouts  79.9 us
    all_to_all x1, blocking collectives, shards(): lax.all_to_all(up_part, 'tp', split_axis=0, concat_axis=2, tiled=True)  52.6 us
    all_to_all x1, local copies, waits for them, and re-layouts, shards(): lax.all_to_all(up_part, 'tp', split_axis=0, concat_axis=2, tiled=True)  49.3 us
  transfers between devices with their start and end apart: 12, of which 9 were waited for; matrix products, arithmetic and copies ran while one was open for 7% of the time, Pallas kernels for 0%

profile of v1, /device:TPU:0, one launch (start us, length us, event | category | flops | bytes accessed | tf_op | source)
XLA Modules:
  0.0 897.0 jit_solution(12534869999038379009)
XLA Ops:
  7.2 8.7 copy.36
  15.9 8.7 copy.39
  24.6 10.7 %multiply_convert_fusion = (bf16[4,256,2048]{1,2,0:T(8,128)(2,1)}, bf16[4,256,2048]{1,2,0:T(8,128)(2,1)}) fusion(f32[4,256,2048]{1,2,0:T(8,128)} %copy.39, f32[256]{0:T(256)S(1)} %copy-done.4, f32[4,256,2048]{1,2,0:T(8,128)} %copy.36), kind=kLoop, calls=%fused_computation.6 | loop fusion | flops 8388608 | bytes 25166848 | tf_op jit(solution)/shard_map/convert_element_type | solution.py:24
  35.3 52.6 %all_to_all.54 = bf16[4,256,2048]{1,2,0:T(8,128)(2,1)S(1)} all-to-all(bf16[4,256,2048]{1,2,0:T(8,128)(2,1)} %get-tuple-element.16), channel_id=1, replica_groups=mesh['fs'=8,'tp'=4] {'tp'}, dimensions={0} | all-to-all | bytes 8388608 | tf_op jit(solution)/shard_map/all_to_all | solution.py:28
  87.9 49.3 %copy.47 = bf16[1,256,8192]{1,0,2:T(2,128)(2,1)} copy(bf16[1,256,8192]{1,2,0:T(8,128)(2,1)S(1)} %bitcast.39) | data formatting | bytes 8388608 | tf_op jit(solution)/shard_map/all_to_all | solution.py:28
  137.7 43.5 %reduce.12 = bf16[8192,256]{1,0:T(8,128)(2,1)} reduce(bf16[8192,1,256]{2,1,0:T(2,128)(2,1)} %bitcast.37, bf16[]{:T(256)} %broadcast.80), dimensions={1}, to_apply=%bitcast.33.reduce_sub_computation | reduce | bytes 8388610
  181.2 6.9 reshape.135
  188.2 99.8 %all_to_all.55 = bf16[8,2,131072]{2,1,0:T(2,128)(2,1)} all-to-all(bf16[8,2,131072]{2,1,0:T(2,128)(2,1)} %reshape.135), channel_id=1, replica_groups=mesh['fs'=8,'tp'=4] {'fs'}, dimensions={0} | all-to-all | bytes 8388608 | tf_op jit(solution)/shard_map/all_to_all | solution.py:32
  288.0 8.7 reshape.136
  296.7 6.1 copy.43
  302.8 6.4 copy.41
  309.3 6.0 convert_element_type.26
  315.4 5.0 all-to-all-start
  320.7 93.3 %all-to-all-done = bf16[4,256,2048]{1,2,0:T(8,128)(2,1)} async-done(((bf16[4,256,2048]{1,2,0:T(8,128)(2,1)}), bf16[4,256,2048]{1,2,0:T(8,128)(2,1)}, u32[]{:S(2)}, u32[]{:S(2)}) %all-to-all-start) | async-done | bytes 4194336 | tf_op jit(solution)/shard_map/all_to_all | solution.py:27
  414.0 6.3 copy.37
  420.3 3.2 fusion.5
  434.3 7.4 collective-permute-done
  442.6 10.4 %collective-permute-done.1 = bf16[1,256,1024]{2,1,0:T(8,128)(2,1)S(1)} collective-permute-done((bf16[1,256,1024]{2,1,0:T(8,128)(2,1)}, bf16[1,256,1024]{2,1,0:T(8,128)(2,1)S(1)}, u32[]{:S(2)}, u32[]{:S(2)}) %collective-permute-start.1) | collective-permute-done | bytes 524320 | tf_op jit(solution)/shard_map/ppermute | solution.py:16
  453.0 11.2 %collective-permute-done.2 = bf16[1,256,1024]{2,1,0:T(8,128)(2,1)S(1)} collective-permute-done((bf16[1,256,1024]{2,1,0:T(8,128)(2,1)}, bf16[1,256,1024]{2,1,0:T(8,128)(2,1)S(1)}, u32[]{:S(2)}, u32[]{:S(2)}) %collective-permute-start.2) | collective-permute-done | bytes 524320 | tf_op jit(solution)/shard_map/ppermute | solution.py:16
  464.2 54.9 %collective-permute-done.3 = bf16[1,256,1024]{2,1,0:T(8,128)(2,1)S(1)} collective-permute-done((bf16[1,256,1024]{2,1,0:T(8,128)(2,1)}, bf16[1,256,1024]{2,1,0:T(8,128)(2,1)S(1)}, u32[]{:S(2)}, u32[]{:S(2)}) %collective-permute-start.3) | collective-permute-done | bytes 524320 | tf_op jit(solution)/shard_map/ppermute | solution.py:16
  529.3 6.3 scatter_custom_fusion
  538.9 8.6 gather_fusion
  547.7 16.2 %fusion = f32[4,480,1024]{2,1,0:T(8,128)} fusion(bf16[4,2048,1024]{2,1,0:T(8,128)(2,1)} %all-gather.6.cloned.1.call-done, bf16[4,480,2048]{2,1,0:T(8,128)(2,1)} %bitcast.44, pred[4,480]{1,0:T(4,128)(4,1)S(1)} %broadcast_in_dim.37), kind=kOutput, calls=%fused_computation.12 | convolution fusion | flops 8056995840 | bytes 32507776 | tf_op jit(solution)/shard_map/ecd,edf->ecf/dot_general | solution.py:66
  565.8 108.1 %all-gather.4.cloned.1.call-done = bf16[4,2048,1024]{2,1,0:T(8,128)(2,1)} async-done(((bf16[1,2048,1024]{2,1,0:T(8,128)(2,1)}), bf16[4,2048,1024]{2,1,0:T(8,128)(2,1)}) %all-gather.4.cloned.1.call-update) | async-done | bytes 16777232 | tf_op jit(solution)/shard_map/all_gather | solution.py:35
  673.9 27.2 %fusion.8 = f32[4,480,2048]{2,1,0:T(8,128)} fusion(bf16[4,1024,2048]{2,1,0:T(8,128)(2,1)} %all-gather.8.cloned.1.call-done, f32[4,480,1024]{2,1,0:T(8,128)} %fusion, bf16[4,2048,1024]{2,1,0:T(8,128)(2,1)} %all-gather.4.cloned.1.call-done, bf16[4,480,2048]{2,1,0:T(8,128)(2,1)} %bitcast.45, pred[4,480]{1,0:T(4,128)(4,1)S(1)} %broadcast_in_dim.37), kind=kOutput, calls=%fused_computation.22 | convolution fusion | flops 16121856000 | bytes 65013632 | tf_op jit(solution)/shard_map/ecf,efd->ecd/dot_general | solution.py:68
  701.1 12.7 %gather_fusion.1 = f32[768,2048]{1,0:T(8,128)} fusion(f32[1920,2048]{1,0:T(8,128)} %bitcast.35, s32[1024]{0:T(1024)S(1)} %get-tuple-element.19), kind=kCustom, calls=%fused_computation.clone | custom fusion | bytes 12585984 | tf_op jit(solution)/shard_map/jit(_take)/gather | solution.py:70
  713.8 12.7 %gather_fusion.2 = f32[768,2048]{1,0:T(8,128)} fusion(f32[1920,2048]{1,0:T(8,128)} %bitcast.36, s32[1024]{0:T(1024)S(1)} %get-tuple-element.18), kind=kCustom, calls=%fused_computation.1.clone | custom fusion | bytes 12585984 | tf_op jit(solution)/shard_map/jit(_take)/gather | solution.py:71
  726.4 7.2 fusion.4
  733.7 118.2 %reduce-scatter.2.cloned.1.call-done = f32[96,2048]{1,0:T(8,128)} async-done(((f32[768,2048]{1,0:T(8,128)}), f32[96,2048]{1,0:T(8,128)}) %reduce-scatter.2.cloned.1.call-update) | async-done | bytes 786448 | tf_op jit(solution)/shard_map/reduce_scatter | solution.py:72
  853.8 15.2 %copy.66 = bf16[4,2048,1024]{2,1,0:T(8,128)(2,1)} copy(bf16[4,2048,1024]{2,1,0:T(8,128)(2,1)} %all-gather.4.cloned.1.call-done) | data formatting | bytes 33554432
  869.0 15.2 %copy.67 = bf16[4,2048,1024]{2,1,0:T(8,128)(2,1)} copy(bf16[4,2048,1024]{2,1,0:T(8,128)(2,1)} %all-gather.6.cloned.1.call-done) | data formatting | bytes 33554432
  884.3 6.2 copy.68
  (86 shorter events, 29.7 us)
Async XLA Ops:
  7.2 540.6 %all-gather.6.cloned.1.call-start = ((), (), s32[]{:S(2)}) async-start(), calls=%async_computation.5 | async-start | bytes 20971520 | tf_op jit(solution)/shard_map/all_gather | solution.py:36
  15.9 8.7 copy-start.4
  309.3 256.5 %all-gather.8.cloned.1.call-start = ((), (), s32[]{:S(2)}) async-start(), calls=%async_computation.6 | async-start | bytes 20971520 | tf_op jit(solution)/shard_map/all_gather | solution.py:38
  315.4 98.6 %all-to-all-start = ((bf16[4,256,2048]{1,2,0:T(8,128)(2,1)}), bf16[4,256,2048]{1,2,0:T(8,128)(2,1)}, u32[]{:S(2)}, u32[]{:S(2)}) async-start(bf16[4,256,2048]{1,2,0:T(8,128)(2,1)} %get-tuple-element.17), calls=%async_computation | async-start | bytes 8388608 | tf_op jit(solution)/shard_map/all_to_all | solution.py:27
  320.4 353.4 %all-gather.4.cloned.1.call-start = ((), (), s32[]{:S(2)}) async-start(), calls=%async_computation.4 | async-start | bytes 20971520 | tf_op jit(solution)/shard_map/all_gather | solution.py:35
  423.5 2.0 copy-start
  427.3 14.4 %collective-permute-start = (bf16[1,256,1024]{2,1,0:T(8,128)(2,1)}, bf16[1,256,1024]{2,1,0:T(8,128)(2,1)S(1)}, u32[]{:S(2)}, u32[]{:S(2)}) collective-permute-start(bf16[1,256,1024]{2,1,0:T(8,128)(2,1)} %get-tuple-element.15), channel_id=1, source_target_pairs={{0,28},{4,0},{8,4},{12,8},{16,12},{20,16},{24,20},{28,24},{1,29},{... | collective-permute-start | bytes 1572872 | tf_op jit(solution)/shard_map/ppermute | solution.py:16
  429.0 23.9 %collective-permute-start.1 = (bf16[1,256,1024]{2,1,0:T(8,128)(2,1)}, bf16[1,256,1024]{2,1,0:T(8,128)(2,1)S(1)}, u32[]{:S(2)}, u32[]{:S(2)}) collective-permute-start(bf16[1,256,1024]{2,1,0:T(8,128)(2,1)} %get-tuple-element.14), channel_id=1, source_target_pairs={{0,24},{4,28},{8,0},{12,4},{16,8},{20,12},{24,16},{28,20},{1,25},{... | collective-permute-start | bytes 1572872 | tf_op jit(solution)/shard_map/ppermute | solution.py:16
  429.0 35.2 %collective-permute-start.2 = (bf16[1,256,1024]{2,1,0:T(8,128)(2,1)}, bf16[1,256,1024]{2,1,0:T(8,128)(2,1)S(1)}, u32[]{:S(2)}, u32[]{:S(2)}) collective-permute-start(bf16[1,256,1024]{2,1,0:T(8,128)(2,1)} %get-tuple-element.13), channel_id=1, source_target_pairs={{0,20},{4,24},{8,28},{12,0},{16,4},{20,8},{24,12},{28,16},{1,21},{... | collective-permute-start | bytes 1572872 | tf_op jit(solution)/shard_map/ppermute | solution.py:16
  430.9 88.2 %collective-permute-start.3 = (bf16[1,256,1024]{2,1,0:T(8,128)(2,1)}, bf16[1,256,1024]{2,1,0:T(8,128)(2,1)S(1)}, u32[]{:S(2)}, u32[]{:S(2)}) collective-permute-start(bf16[1,256,1024]{2,1,0:T(8,128)(2,1)} %get-tuple-element.12), channel_id=1, source_target_pairs={{0,16},{4,20},{8,24},{12,28},{16,0},{20,4},{24,8},{28,12},{1,17},{... | collective-permute-start | bytes 1572872 | tf_op jit(solution)/shard_map/ppermute | solution.py:16
  432.0 88.9 %collective-permute-start.4 = (bf16[1,256,1024]{2,1,0:T(8,128)(2,1)}, bf16[1,256,1024]{2,1,0:T(8,128)(2,1)S(1)}, u32[]{:S(2)}, u32[]{:S(2)}) collective-permute-start(bf16[1,256,1024]{2,1,0:T(8,128)(2,1)} %get-tuple-element.11), channel_id=1, source_target_pairs={{0,12},{4,16},{8,20},{12,24},{16,28},{20,0},{24,4},{28,8},{1,13},{... | collective-permute-start | bytes 1572872 | tf_op jit(solution)/shard_map/ppermute | solution.py:16
  441.7 79.2 %collective-permute-start.5 = (bf16[1,256,1024]{2,1,0:T(8,128)(2,1)}, bf16[1,256,1024]{2,1,0:T(8,128)(2,1)S(1)}, u32[]{:S(2)}, u32[]{:S(2)}) collective-permute-start(bf16[1,256,1024]{2,1,0:T(8,128)(2,1)} %get-tuple-element.10), channel_id=1, source_target_pairs={{0,8},{4,12},{8,16},{12,20},{16,24},{20,28},{24,0},{28,4},{1,9},{5... | collective-permute-start | bytes 1572872 | tf_op jit(solution)/shard_map/ppermute | solution.py:16
  452.9 68.1 %collective-permute-start.6 = (bf16[1,256,1024]{2,1,0:T(8,128)(2,1)S(1)}, bf16[1,256,1024]{2,1,0:T(8,128)(2,1)S(1)}, u32[]{:S(2)}, u32[]{:S(2)}) collective-permute-start(bf16[1,256,1024]{2,1,0:T(8,128)(2,1)S(1)} %get-tuple-element.9), channel_id=1, source_target_pairs={{0,4},{4,8},{8,12},{12,16},{16,20},{20,24},{24,28},{28,0},{1,5},{5... | collective-permute-start | bytes 1572872 | tf_op jit(solution)/shard_map/ppermute | solution.py:16
  522.3 3.9 copy-start.2
  522.4 13.4 %copy-start.1 = (bf16[768,2048]{1,0:T(8,128)(2,1)S(1)}, bf16[768,2048]{1,0:T(8,128)(2,1)}, u32[]{:S(2)}) copy-start(bf16[768,2048]{1,0:T(8,128)(2,1)} %param.9) | copy-start | bytes 9437188
  526.2 325.7 %reduce-scatter.2.cloned.1.call-start = ((), (), s32[]{:S(2)}) async-start(), calls=%async_computation.7 | async-start | bytes 7077888 | tf_op jit(solution)/shard_map/reduce_scatter | solution.py:72
  538.9 8.7 copy-start.3
  853.8 30.5 %slice-start = ((s8[16777216]{0:T(1024)(128)(4,1)}), s8[4194304]{0:T(1024)(128)(4,1)S(1)}, s32[]{:S(2)}) async-start(s8[16777216]{0:T(1024)(128)(4,1)} %bitcast.41), calls=%async_computation.8 | async-start | bytes 8388608
  853.8 30.5 %slice-start.1 = ((s8[16777216]{0:T(1024)(128)(4,1)}), s8[4194304]{0:T(1024)(128)(4,1)S(1)}, s32[]{:S(2)}) async-start(s8[16777216]{0:T(1024)(128)(4,1)} %bitcast.41), calls=%async_computation.9 | async-start | bytes 8388608
  869.0 15.2 %slice-start.2 = ((s8[16777216]{0:T(1024)(128)(4,1)}), s8[4194304]{0:T(1024)(128)(4,1)S(1)}, s32[]{:S(2)}) async-start(s8[16777216]{0:T(1024)(128)(4,1)} %bitcast.41), calls=%async_computation.10 | async-start | bytes 8388608
  869.0 15.2 %slice-start.3 = ((s8[16777216]{0:T(1024)(128)(4,1)}), s8[4194304]{0:T(1024)(128)(4,1)S(1)}, s32[]{:S(2)}) async-start(s8[16777216]{0:T(1024)(128)(4,1)} %bitcast.41), calls=%async_computation.11 | async-start | bytes 8388608
Sparse Core Ops, SparseCore 0:
  309.4 148.9 all-gather.5
  460.0 105.7 all-gather.7
  567.9 105.8 all-gather.3
  733.8 118.0 reduce-scatter.1
